TPU v7x, 32 devices: a whole 2x2x4 slice. The times are simulated.
32 devices in a mesh: grp: 2 (over y), ep: 4 (over z), tp: 4 (over x, core).
Axes of the slice: x: 2, y: 2, z: 4, core: 2. Of those that a mesh axis runs over, the one named last changes fastest.
Arguments:
- mix_input: bfloat16 [2048, 2048], P(('grp', 'ep'), 'tp'), parts along dimension 0, may hold values from -6 to 6
- group_weight: bfloat16 [16, 128, 128], replicated, may hold values from -0.5 to 0.5
- pool_gain: float32 [2048], replicated, may hold values from 0.1 to 1.9
- branch_weight: bfloat16 [2048, 2048], P('tp'), may hold values from -0.125 to 0.125
- exp_input: bfloat16 [1024, 2048], P(('grp', 'ep')), parts along dimension 0, may hold values from -6 to 6
- norm_gain: float32 [2048], replicated, may hold values from 0.1 to 1.9
- routes: int32 [1024, 2], P(('grp', 'ep')), parts along dimension 0, may hold values from 0 to 3, all different within a row; in each aligned block of 128 rows (0 to 127, 128 to 255, ...) at most 96 rows name the same one
- route_weights: float32 [1024, 2], P(('grp', 'ep')), parts along dimension 0, may hold values from 0.25 to 1
- gate_weight: bfloat16 [4, 2048, 3584], P('ep', None, 'tp'), may hold values from -0.125 to 0.125
- up_weight: bfloat16 [4, 2048, 3584], P('ep', None, 'tp'), may hold values from -0.125 to 0.125
- down_weight: bfloat16 [4, 3584, 2048], P('ep', 'tp'), may hold values from -0.09375 to 0.09375
Outputs:
- mix_out: bfloat16 [2048, 2048], P(('grp', 'ep'), 'tp'), parts along dimension 0
- exp_out: bfloat16 [1024, 2048], P(('grp', 'ep'), 'tp'), parts along dimension 0
There are 2 independent parts, one for each index of `grp`. A program takes and returns all parts, laid end to end along the dimension named above; an argument that names none is the same for every part. Nothing has to cross between parts.
Inputs may be any that keep to these rules, and one draw needn't show every extreme that they name: `routes`: the 2 experts of a token differ. Among the 128 tokens of one index of ep no expert is named by more than 96 of them, a bound that some block reaches.
All inputs are finite; a program needn't handle non-finite values.
Results may differ from a plain program's by a relative error of at most 0.018.
Values may be sent and summed in bfloat16 or wider, within the bound.
No kernel may reach another device: no remote copies, remote signals or barrier semaphores. Data moves between devices by JAX's collectives and lax.ppermute only.
A program may use at most 64 MiB of HBM per device.

v0:
```python
import jax
import jax.numpy as jnp
from jax import lax
from jax.experimental import pallas as pl
from jax.experimental.pallas import tpu as pltpu
from jax.sharding import PartitionSpec as P

windows = (2, 4, 8, 16)
epsilon = 1e-06
halo = 16
f32, bf16 = jnp.float32, jnp.bfloat16
params = pltpu.CompilerParams(vmem_limit_bytes=24 * 2**20)


def shifted(block, axis, distance):
    devices = range(lax.axis_size(axis))
    route = [(i - distance, i) for i in devices if i - distance in devices]
    return lax.ppermute(block, axis, route)


def rotated(block, axis, distance):
    count = lax.axis_size(axis)
    return lax.ppermute(block, axis, [(i, (i + distance) % count) for i in range(count)])


def paired(block):
    count = lax.axis_size("tp")
    return lax.ppermute(block, "tp", [(i, i ^ 1) for i in range(count)])


def ranks_of(routes, ep_rank, experts):
    tokens, top = routes.shape
    relative = lax.rem(ep_rank + lax.broadcasted_iota(jnp.int32, (tokens, experts), 1), experts)
    hits = [(routes[:, k : k + 1] == relative) for k in range(top)]
    member = sum(jnp.where(h, 1.0, 0.0) for h in hits)
    row = lax.broadcasted_iota(jnp.int32, (tokens, tokens), 0)
    col = lax.broadcasted_iota(jnp.int32, (tokens, tokens), 1)
    before = jnp.where(col < row, 1.0, 0.0).astype(bf16)
    rank = jnp.dot(before, member.astype(bf16), preferred_element_type=f32)
    return [jnp.where(h, rank, -1.0) for h in hits], jnp.where(member > 0.5, rank, -1.0)


def prepare(scalars, exp_input, norm_gain, routes, order, capacity):
    tokens, width = exp_input.shape
    half = width // 2
    experts = len(order)
    top = routes.shape[1]

    def body(scal, x_ref, gain_ref, routes_ref, *outs):
        floated = x_ref[...].astype(f32)
        scale = lax.rsqrt(jnp.mean(floated * floated, axis=1, keepdims=True) + epsilon)
        low = (floated[:, :half] * scale * gain_ref[:, :half]).astype(bf16)
        high = (floated[:, half:] * scale * gain_ref[:, half:]).astype(bf16)
        mine = jnp.where(lax.rem(scal[0], 2) == 0, low, high)
        relative = lax.rem(
            scal[1] + lax.broadcasted_iota(jnp.int32, (experts, tokens), 0), experts
        )
        member = sum(
            jnp.where(routes_ref[k : k + 1, :] == relative, 1.0, 0.0) for k in range(top)
        )
        row = lax.broadcasted_iota(jnp.int32, (tokens, tokens), 0)
        col = lax.broadcasted_iota(jnp.int32, (tokens, tokens), 1)
        earlier = jnp.where(row < col, 1.0, 0.0).astype(bf16)
        rank = jnp.dot(member.astype(bf16), earlier, preferred_element_type=f32)
        place = jnp.where(member > 0.5, rank, -1.0)
        slots = lax.broadcasted_iota(jnp.int32, (capacity, tokens), 0).astype(f32)
        for out, k in zip(outs, order):
            pick = jnp.where(place[k : k + 1, :] == slots, 1.0, 0.0).astype(bf16)
            out[...] = jnp.dot(pick, mine, preferred_element_type=f32).astype(bf16)

    return pl.pallas_call(
        body,
        in_specs=[
            pl.BlockSpec(memory_space=pltpu.SMEM),
            pl.BlockSpec(memory_space=pltpu.VMEM),
            pl.BlockSpec(memory_space=pltpu.VMEM),
            pl.BlockSpec(memory_space=pltpu.VMEM),
        ],
        out_specs=[pl.BlockSpec(memory_space=pltpu.VMEM)] * experts,
        out_shape=[jax.ShapeDtypeStruct((capacity, half), bf16)] * experts,
        name="prepare",
        compiler_params=params,
    )(scalars, exp_input, norm_gain.reshape(1, width), routes.T)


def combine(scalars, routes, route_weights, chunks, order):
    tokens, top = routes.shape
    capacity, columns = chunks[0].shape
    experts = len(order)

    def body(scal, routes_ref, weights_ref, *refs):
        out = refs[-1]
        places, _ = ranks_of(routes_ref[...], scal[1], experts)
        slots = lax.broadcasted_iota(jnp.int32, (tokens, capacity), 1).astype(f32)
        total = jnp.zeros((tokens, columns), f32)
        for k in range(top):
            chosen = jnp.zeros((tokens, columns), f32)
            for ref, e in zip(refs, order):
                pick = jnp.where(places[k][:, e : e + 1] == slots, 1.0, 0.0).astype(bf16)
                chosen = chosen + jnp.dot(pick, ref[...], preferred_element_type=f32)
            total = total + chosen * weights_ref[:, k : k + 1]
        out[...] = total.astype(bf16)

    return pl.pallas_call(
        body,
        in_specs=[pl.BlockSpec(memory_space=pltpu.SMEM)]
        + [pl.BlockSpec(memory_space=pltpu.VMEM)] * (2 + experts),
        out_specs=pl.BlockSpec(memory_space=pltpu.VMEM),
        out_shape=jax.ShapeDtypeStruct((tokens, columns), bf16),
        name="combine",
        compiler_params=params,
    )(scalars, routes, route_weights, *chunks)


def column_block(step, rank, chips):
    core, chip = lax.rem(rank, 2), lax.div(rank, 2)
    place = lax.rem(chip + step % chips, chips)
    return 2 * place + (1 - core if step < chips else core)


def mixer(scalars, mix_input, before, group_weight, pool_gain, branch_weight, members):
    rows, channels = mix_input.shape
    group_width = group_weight.shape[1]
    group_count = channels // group_width
    width = branch_weight.shape[1]
    columns = width // members
    chips = members // 2

    def body(scal, x_hbm, before_ref, group_hbm, gain_ref, branch_hbm, give_ref, keep_ref,
             x_ref, group_ref, branch_ref, pooled, sems):
        copies = [
            pltpu.make_async_copy(x_hbm, x_ref, sems.at[0]),
            pltpu.make_async_copy(
                group_hbm.at[pl.ds(scal[0] * group_count, group_count)], group_ref, sems.at[1]
            ),
            pltpu.make_async_copy(branch_hbm, branch_ref, sems.at[2]),
        ]
        for copy in copies:
            copy.start()
        copies[0].wait()
        copies[1].wait()
        place = scal[1] * rows + lax.broadcasted_iota(jnp.int32, (rows, group_width), 0)
        for g in range(group_count):
            cut = slice(g * group_width, (g + 1) * group_width)
            extended = jnp.concatenate(
                [before_ref[:, cut].astype(f32), x_ref[:, cut].astype(f32)], axis=0
            )
            level = lax.rem(scal[0] * group_count + g, len(windows))
            sums = extended
            chosen = jnp.zeros_like(extended)
            for index, window in enumerate(windows):
                sums = sums + pltpu.roll(sums, window // 2, 0)
                chosen = jnp.where(level == index, sums, chosen)
            length = lax.shift_left(jnp.int32(2), level)
            counted = jnp.minimum(place + 1, length).astype(f32)
            deviation = (chosen[halo:] / counted - extended[halo:]).astype(bf16)
            grouped = jnp.dot(deviation, group_ref[g], preferred_element_type=f32)
            at = pl.multiple_of(scal[0] * channels + g * group_width, 128)
            pooled[:, cut] = (grouped * gain_ref[:, pl.ds(at, group_width)]).astype(bf16)
        copies[2].wait()
        for step in range(members):
            at = pl.multiple_of(column_block(step, scal[0], chips) * columns, 128)
            result = jnp.dot(
                pooled[...], branch_ref[:, pl.ds(at, columns)], preferred_element_type=f32
            ).astype(bf16)
            if step < chips:
                give_ref[step] = result
            else:
                keep_ref[step - chips] = result

    vmem = pl.BlockSpec(memory_space=pltpu.VMEM)
    hbm = pl.BlockSpec(memory_space=pltpu.HBM)
    return pl.pallas_call(
        body,
        in_specs=[pl.BlockSpec(memory_space=pltpu.SMEM), hbm, vmem, hbm, vmem, hbm],
        out_specs=[vmem, vmem],
        scratch_shapes=[
            pltpu.VMEM((rows, channels), bf16),
            pltpu.VMEM((group_count, group_width, group_width), bf16),
            pltpu.VMEM(branch_weight.shape, bf16),
            pltpu.VMEM((rows, channels), bf16),
            pltpu.SemaphoreType.DMA((3,)),
        ],
        out_shape=[jax.ShapeDtypeStruct((chips, rows, columns), bf16)] * 2,
        name="mixer",
        compiler_params=params,
    )(scalars, mix_input, before, group_weight, pool_gain.reshape(1, -1), branch_weight)


def load(*weights):
    count = len(weights)

    def body(*refs):
        sems = refs[-1]
        copies = [
            pltpu.make_async_copy(refs[i], refs[count + i], sems.at[i]) for i in range(count)
        ]
        for copy in copies:
            copy.start()
        for copy in copies:
            copy.wait()

    return pl.pallas_call(
        body,
        in_specs=[pl.BlockSpec(memory_space=pltpu.HBM)] * count,
        out_specs=[pl.BlockSpec(memory_space=pl.ANY)] * count,
        out_shape=[jax.ShapeDtypeStruct(w.shape, w.dtype) for w in weights],
        scratch_shapes=[pltpu.SemaphoreType.DMA((count,))],
        name="load",
        compiler_params=params,
    )(*weights)


def whole_call(body, shapes, scalars, *arrays):
    vmem = pl.BlockSpec(memory_space=pltpu.VMEM)
    return pl.pallas_call(
        body,
        in_specs=[pl.BlockSpec(memory_space=pltpu.SMEM)] + [vmem] * len(arrays),
        out_specs=[vmem] * len(shapes),
        out_shape=shapes,
        compiler_params=params,
    )(scalars, *arrays)


def enter(scalars, mine, gate_weight, up_weight):
    rows, half = mine.shape
    shape = jax.ShapeDtypeStruct((rows, gate_weight.shape[2]), f32)

    def body(scal, mine_ref, gate_ref, up_ref, gate, up):
        at = pl.ds(pl.multiple_of(lax.rem(scal[0], 2) * half, 128), half)
        gate[...] = jnp.dot(mine_ref[...], gate_ref[0, at, :], preferred_element_type=f32)
        up[...] = jnp.dot(mine_ref[...], up_ref[0, at, :], preferred_element_type=f32)

    return whole_call(body, [shape, shape], scalars, mine, gate_weight, up_weight)


def middle(scalars, theirs, gate_weight, up_weight, gate, up, down_weight, members):
    rows, half = theirs.shape
    hidden_size, width = down_weight.shape[1:]
    columns, chips = width // members, members // 2

    def body(scal, theirs_ref, gate_ref, up_ref, gate_acc, up_acc, down_ref, hidden, give):
        at = pl.ds(pl.multiple_of((1 - lax.rem(scal[0], 2)) * half, 128), half)
        value = gate_acc[...] + jnp.dot(
            theirs_ref[...], gate_ref[0, at, :], preferred_element_type=f32
        )
        other = up_acc[...] + jnp.dot(
            theirs_ref[...], up_ref[0, at, :], preferred_element_type=f32
        )
        hidden[...] = (value / (1.0 + jnp.exp(-value)) * other).astype(bf16)
        for step in range(chips):
            col = pl.multiple_of(column_block(step, scal[0], chips) * columns, 128)
            give[step] = jnp.dot(
                hidden[...], down_ref[0, :, pl.ds(col, columns)], preferred_element_type=f32
            ).astype(bf16)

    shapes = [
        jax.ShapeDtypeStruct((rows, hidden_size), bf16),
        jax.ShapeDtypeStruct((chips, rows, columns), bf16),
    ]
    return whole_call(body, shapes, scalars, theirs, gate_weight, up_weight, gate, up, down_weight)


def leave(scalars, hidden, down_weight, members):
    rows = hidden.shape[0]
    columns, chips = down_weight.shape[2] // members, members // 2

    def body(scal, hidden_ref, down_ref, keep):
        for step in range(chips):
            col = pl.multiple_of(column_block(chips + step, scal[0], chips) * columns, 128)
            keep[step] = jnp.dot(
                hidden_ref[...], down_ref[0, :, pl.ds(col, columns)], preferred_element_type=f32
            ).astype(bf16)

    shape = jax.ShapeDtypeStruct((chips, rows, columns), bf16)
    return whole_call(body, [shape], scalars, hidden, down_weight)[0]


def reduced(got, keep, cuts):
    chips = keep.shape[0]
    pieces = []
    for start, stop in cuts:
        part = [
            (keep[r, start:stop].astype(f32) + got[r, start:stop].astype(f32)).astype(bf16)
            for r in range(chips)
        ]
        total = part[0].astype(f32)
        for r in range(1, chips):
            moved = rotated(part[r], "tp", 2 * r)
            total = total + moved.astype(f32)
        pieces.append(total.astype(bf16))
    return pieces


def layer(
    mix_input,
    group_weight,
    pool_gain,
    branch_weight,
    exp_input,
    norm_gain,
    routes,
    route_weights,
    gate_weight,
    up_weight,
    down_weight,
):
    members = lax.axis_size("tp")
    experts = lax.axis_size("ep")
    scalars = jnp.stack([lax.axis_index("tp"), lax.axis_index("ep")]).astype(jnp.int32)
    rows_mix = mix_input.shape[0]
    capacity = 3 * exp_input.shape[0] // experts
    order = sorted(range(1, experts), key=lambda k: -min(k, experts - k)) + [0]
    outgoing = prepare(scalars, exp_input, norm_gain, routes, order, capacity)
    *outgoing, late_mix = lax.optimization_barrier((*outgoing, mix_input))
    arrivals = []
    for block, k in zip(outgoing[:-1], order):
        arrivals.append(rotated(block, "ep", k))
    before = shifted(late_mix[rows_mix - halo :], "ep", 1)
    give, keep = mixer(scalars, mix_input, before, group_weight, pool_gain, branch_weight, members)
    got = paired(give)
    (mix_out,) = reduced(got, keep, [(0, rows_mix)])
    gate_weight, up_weight, down_weight = load(gate_weight, up_weight, down_weight)
    *arrivals, mix_out = lax.optimization_barrier((*arrivals, mix_out))
    mine = jnp.concatenate([*arrivals, outgoing[-1]], axis=0)
    theirs = paired(mine)
    gate, up = enter(scalars, mine, gate_weight, up_weight)
    hidden, give = middle(scalars, theirs, gate_weight, up_weight, gate, up, down_weight, members)
    got = paired(give)
    keep = leave(scalars, hidden, down_weight, members)
    groups = [order[:1], order[1:-1], order[-1:]]
    cuts, at = [], 0
    for group in groups:
        cuts.append((at, at + capacity * len(group)))
        at += capacity * len(group)
    chunks = []
    for group, piece in zip(groups, reduced(got, keep, cuts)):
        for j, k in enumerate(group):
            part = piece[j * capacity : (j + 1) * capacity]
            chunks.append(rotated(part, "ep", -k) if k else part)
    exp_out = combine(scalars, routes, route_weights, chunks, order)
    return (mix_out, exp_out)


def solution(mesh):
    return jax.shard_map(
        layer,
        mesh=mesh,
        in_specs=(
            P(("grp", "ep"), "tp"),
            P(),
            P(),
            P("tp", None),
            P(("grp", "ep"), None),
            P(),
            P(("grp", "ep"), None),
            P(("grp", "ep"), None),
            P("ep", None, "tp"),
            P("ep", None, "tp"),
            P("ep", "tp", None),
        ),
        out_specs=(P(("grp", "ep"), "tp"), P(("grp", "ep"), "tp")),
        check_vma=False,
    )
```

profile of v0, /device:TPU:0, one launch (start us, length us, event | category | flops | bytes accessed | tf_op | source)
XLA Modules:
  0.0 77.6 jit_solution(14627974792810590277)
XLA Ops:
  0.7 1.2 %copy-done.5 = bf16[128,2048]{1,0:T(8,128)(2,1)S(1)} copy-done((bf16[128,2048]{1,0:T(8,128)(2,1)S(1)}, bf16[128,2048]{1,0:T(8,128)(2,1)}, u32[]{:S(2)}) %copy-start.5) | copy-done | bytes 524312
  3.3 1.1 %prepare.1 = (bf16[96,1024]{1,0:T(8,128)(2,1)S(1)}, bf16[96,1024]{1,0:T(8,128)(2,1)S(1)}, bf16[96,1024]{1,0:T(8,128)(2,1)S(1)}, bf16[96,1024]{1,0:T(8,128)(2,1)S(1)}) custom-call(s32[2]{0:T(128)S(1)} %pad_add_fusion.scal, bf16[128,2048]{1,0:T(8,128)(2,1)S(1)} %copy-done.5, f32[1,2048]{1,0:T(1,128)S(1)} %bitcast.33, s32[2,128]{1,0:T(2,128)S(1)} %bitcast.35), custom_call_target="tpu_custom_call" | custom-call | tf_op jit(solution)/shard_map/prepare/pallas_call | solution.py:71
  4.4 0.7 slice.57
  5.1 4.9 %collective-permute-start.3 = (bf16[16,512]{1,0:T(8,128)(2,1)S(1)}, bf16[16,512]{1,0:T(8,128)(2,1)S(1)}, u32[]{:S(2)}, u32[]{:S(2)}) collective-permute-start(bf16[16,512]{1,0:T(8,128)(2,1)S(1)} %slice.57), channel_id=1, source_target_pairs={{0,4},{4,8},{8,12},{1,5},{5,9},{9,13},{2,6},{6,10},{10,14},{3,7},{... | collective-permute-start | bytes 49160 | tf_op jit(solution)/shard_map/ppermute | solution.py:18
  10.1 1.4 %collective-permute-done.3.before_ref = bf16[16,512]{1,0:T(8,128)(2,1)S(1)} collective-permute-done((bf16[16,512]{1,0:T(8,128)(2,1)S(1)}, bf16[16,512]{1,0:T(8,128)(2,1)S(1)}, u32[]{:S(2)}, u32[]{:S(2)}) %collective-permute-start.3) | collective-permute-done | bytes 16416 | tf_op jit(solution)/shard_map/ppermute | solution.py:18
  11.5 1.6 %copy-done.3 = bf16[512,2048]{1,0:T(8,128)(2,1)S(1)} copy-done((bf16[512,2048]{1,0:T(8,128)(2,1)S(1)}, bf16[512,2048]{1,0:T(8,128)(2,1)}, u32[]{:S(2)}) %copy-start.3) | copy-done | bytes 2097176
  13.1 1.0 %copy-done.4 = bf16[16,128,128]{2,1,0:T(8,128)(2,1)S(1)} copy-done((bf16[16,128,128]{2,1,0:T(8,128)(2,1)S(1)}, bf16[16,128,128]{2,1,0:T(8,128)(2,1)}, u32[]{:S(2)}) %copy-start.4) | copy-done | bytes 524312
  14.1 0.9 %copy-done.6 = bf16[256,512]{1,0:T(8,128)(2,1)S(1)} copy-done((bf16[256,512]{1,0:T(8,128)(2,1)S(1)}, bf16[256,512]{1,0:T(8,128)(2,1)}, u32[]{:S(2)}) %copy-start.6) | copy-done | bytes 262168
  15.8 2.2 %mixer.1 = (bf16[2,256,512]{2,1,0:T(8,128)(2,1)S(1)}, bf16[2,256,512]{2,1,0:T(8,128)(2,1)S(1)}) custom-call(s32[2]{0:T(128)S(1)} %pad_add_fusion.scal, bf16[256,512]{1,0:T(8,128)(2,1)S(1)} %copy-done.6, bf16[16,512]{1,0:T(8,128)(2,1)S(1)} %collective-permute-done.3.before_ref, bf16[16,128,128]{2,1,0:T(8,128)(2,1)S(1)} %copy-done.4, f32[1,2048]{1,0:T(1,128)S(1)} %bitcast.34, ...), custom_call_target="tpu_custom_call" | custom-call | tf_op jit(solution)/shard_map/mixer/pallas_call | solution.py:173
  18.0 1.9 %collective-permute-done.4 = bf16[2,256,512]{2,1,0:T(8,128)(2,1)S(1)} collective-permute-done((bf16[2,256,512]{2,1,0:T(8,128)(2,1)S(1)}, bf16[2,256,512]{2,1,0:T(8,128)(2,1)S(1)}, u32[]{:S(2)}, u32[]{:S(2)}) %collective-permute-start.4) | collective-permute-done | bytes 524320 | tf_op jit(solution)/shard_map/ppermute | solution.py:28
  20.0 1.6 %collective-permute-start.5 = (bf16[256,512]{1,0:T(8,128)(2,1)S(1)}, bf16[256,512]{1,0:T(8,128)(2,1)S(1)}, u32[]{:S(2)}, u32[]{:S(2)}) collective-permute-start(bf16[256,512]{1,0:T(8,128)(2,1)S(1)} %fusion.3), channel_id=1, source_target_pairs={{0,2},{1,3},{2,0},{3,1},{4,6},{5,7},{6,4},{7,5},{8,10},{9,11},{10,... | collective-permute-start | bytes 786440 | tf_op jit(solution)/shard_map/ppermute | solution.py:23
  21.6 3.3 %collective-permute-start = (bf16[96,1024]{1,0:T(8,128)(2,1)S(1)}, bf16[96,1024]{1,0:T(8,128)(2,1)S(1)}, u32[]{:S(2)}, u32[]{:S(2)}) collective-permute-start(bf16[96,1024]{1,0:T(8,128)(2,1)S(1)} %get-tuple-element.28), channel_id=1, source_target_pairs={{0,8},{4,12},{8,0},{12,4},{1,9},{5,13},{9,1},{13,5},{2,10},{6,14},... | collective-permute-start | bytes 589832 | tf_op jit(solution)/shard_map/ppermute | solution.py:23
  24.9 1.6 %collective-permute-start.1 = (bf16[96,1024]{1,0:T(8,128)(2,1)S(1)}, bf16[96,1024]{1,0:T(8,128)(2,1)S(1)}, u32[]{:S(2)}, u32[]{:S(2)}) collective-permute-start(bf16[96,1024]{1,0:T(8,128)(2,1)S(1)} %get-tuple-element.29), channel_id=1, source_target_pairs={{0,4},{4,8},{8,12},{12,0},{1,5},{5,9},{9,13},{13,1},{2,6},{6,10},{... | collective-permute-start | bytes 589832 | tf_op jit(solution)/shard_map/ppermute | solution.py:23
  26.4 2.2 %collective-permute-start.2 = (bf16[96,1024]{1,0:T(8,128)(2,1)S(1)}, bf16[96,1024]{1,0:T(8,128)(2,1)S(1)}, u32[]{:S(2)}, u32[]{:S(2)}) collective-permute-start(bf16[96,1024]{1,0:T(8,128)(2,1)S(1)} %get-tuple-element.30), channel_id=1, source_target_pairs={{0,12},{4,0},{8,4},{12,8},{1,13},{5,1},{9,5},{13,9},{2,14},{6,2},{... | collective-permute-start | bytes 589832 | tf_op jit(solution)/shard_map/ppermute | solution.py:23
  28.7 0.8 %fusion = bf16[256,512]{1,0:T(8,128)(2,1)} fusion(bf16[256,512]{1,0:T(8,128)(2,1)S(1)} %collective-permute-done.5, bf16[2,256,512]{2,1,0:T(8,128)(2,1)S(1)} %collective-permute-done.4, bf16[2,256,512]{2,1,0:T(8,128)(2,1)S(1)} %get-tuple-element.32), kind=kLoop, calls=%fused_computation.1 | loop fusion | flops 1048576 | bytes 1048576 | tf_op jit(solution)/shard_map/convert_element_type | solution.py:291
  29.5 9.6 %collective-permute-done = bf16[96,1024]{1,0:T(8,128)(2,1)S(1)} collective-permute-done((bf16[96,1024]{1,0:T(8,128)(2,1)S(1)}, bf16[96,1024]{1,0:T(8,128)(2,1)S(1)}, u32[]{:S(2)}, u32[]{:S(2)}) %collective-permute-start) | collective-permute-done | bytes 196640 | tf_op jit(solution)/shard_map/ppermute | solution.py:23
  39.1 0.7 collective-permute-done.2
  40.0 2.0 %copy-done.1 = bf16[1,2048,896]{2,1,0:T(8,128)(2,1)S(1)} copy-done((bf16[1,2048,896]{2,1,0:T(8,128)(2,1)S(1)}, bf16[1,2048,896]{2,1,0:T(8,128)(2,1)}, u32[]{:S(2)}) %copy-start.1) | copy-done | bytes 3670040
  42.0 2.0 %copy-done.2 = bf16[1,896,2048]{2,1,0:T(8,128)(2,1)S(1)} copy-done((bf16[1,896,2048]{2,1,0:T(8,128)(2,1)S(1)}, bf16[1,896,2048]{2,1,0:T(8,128)(2,1)}, u32[]{:S(2)}) %copy-start.2) | copy-done | bytes 3670040
  44.1 0.8 load.1
  44.8 2.3 %shard_map.122 = (f32[384,896]{1,0:T(8,128)S(1)}, f32[384,896]{1,0:T(8,128)S(1)}) custom-call(s32[2]{0:T(128)S(1)} %pad_add_fusion.scal, bf16[384,1024]{1,0:T(8,128)(2,1)S(1)} %constant_dynamic-update-slice_fusion.mine_ref, bf16[1,2048,896]{2,1,0:T(8,128)(2,1)S(1)} %get-tuple-element.39.gate_ref, bf16[1,2048,896]{2,1,0:T(8,128)(2,1)S(1)} %get-tuple-element.40.up_ref), custom_call_target="tpu_custom_call" | custom-call | tf_op jit(solution)/shard_map/pallas_call | solution.py:216
  47.2 3.4 %shard_map.123 = (bf16[384,896]{1,0:T(8,128)(2,1)S(1)}, bf16[2,384,512]{2,1,0:T(8,128)(2,1)S(1)}) custom-call(s32[2]{0:T(128)S(1)} %pad_add_fusion.scal, bf16[384,1024]{1,0:T(8,128)(2,1)S(1)} %collective-permute-done.6.theirs_ref, bf16[1,2048,896]{2,1,0:T(8,128)(2,1)S(1)} %get-tuple-element.39.gate_ref, bf16[1,2048,896]{2,1,0:T(8,128)(2,1)S(1)} %get-tuple-element.40.up_ref, ...), custom_call_target="tpu_custom_call" | custom-call | tf_op jit(solution)/shard_map/pallas_call | solution.py:216
  51.1 1.5 %shard_map.124 = bf16[2,384,512]{2,1,0:T(8,128)(2,1)S(1)} custom-call(s32[2]{0:T(128)S(1)} %pad_add_fusion.scal, bf16[384,896]{1,0:T(8,128)(2,1)S(1)} %get-tuple-element.44.hidden_ref, bf16[1,896,2048]{2,1,0:T(8,128)(2,1)S(1)} %get-tuple-element.43.down_ref), custom_call_target="tpu_custom_call" | custom-call | tf_op jit(solution)/shard_map/pallas_call | solution.py:216
  53.7 1.5 %collective-permute-start.8 = (bf16[96,512]{1,0:T(8,128)(2,1)S(1)}, bf16[96,512]{1,0:T(8,128)(2,1)S(1)}, u32[]{:S(2)}, u32[]{:S(2)}) collective-permute-start(bf16[96,512]{1,0:T(8,128)(2,1)S(1)} %get-tuple-element.49), channel_id=1, source_target_pairs={{0,2},{1,3},{2,0},{3,1},{4,6},{5,7},{6,4},{7,5},{8,10},{9,11},{10,... | collective-permute-start | bytes 294920 | tf_op jit(solution)/shard_map/ppermute | solution.py:23
  55.8 3.0 %collective-permute-done.13 = bf16[96,512]{1,0:T(8,128)(2,1)S(1)} collective-permute-done((bf16[96,512]{1,0:T(8,128)(2,1)S(1)}, bf16[96,512]{1,0:T(8,128)(2,1)S(1)}, u32[]{:S(2)}, u32[]{:S(2)}) %collective-permute-start.13) | collective-permute-done | bytes 98336 | tf_op jit(solution)/shard_map/ppermute | solution.py:23
  58.8 2.1 %collective-permute-done.8 = bf16[96,512]{1,0:T(8,128)(2,1)S(1)} collective-permute-done((bf16[96,512]{1,0:T(8,128)(2,1)S(1)}, bf16[96,512]{1,0:T(8,128)(2,1)S(1)}, u32[]{:S(2)}, u32[]{:S(2)}) %collective-permute-start.8) | collective-permute-done | bytes 98336 | tf_op jit(solution)/shard_map/ppermute | solution.py:23
  61.0 5.3 %collective-permute-start.9 = (bf16[96,512]{1,0:T(8,128)(2,1)S(1)}, bf16[96,512]{1,0:T(8,128)(2,1)S(1)}, u32[]{:S(2)}, u32[]{:S(2)}) collective-permute-start(bf16[96,512]{1,0:T(8,128)(2,1)S(1)} %get-tuple-element.47), channel_id=1, source_target_pairs={{0,8},{4,12},{8,0},{12,4},{1,9},{5,13},{9,1},{13,5},{2,10},{6,14},... | collective-permute-start | bytes 294920 | tf_op jit(solution)/shard_map/ppermute | solution.py:23
  66.9 1.6 %collective-permute-start.12 = (bf16[96,512]{1,0:T(8,128)(2,1)S(1)}, bf16[96,512]{1,0:T(8,128)(2,1)S(1)}, u32[]{:S(2)}, u32[]{:S(2)}) collective-permute-start(bf16[96,512]{1,0:T(8,128)(2,1)S(1)} %get-tuple-element.50), channel_id=1, source_target_pairs={{0,4},{4,8},{8,12},{12,0},{1,5},{5,9},{9,13},{13,1},{2,6},{6,10},{... | collective-permute-start | bytes 294920 | tf_op jit(solution)/shard_map/ppermute | solution.py:23
  68.7 1.6 %collective-permute-done.9.refs_0_ = bf16[96,512]{1,0:T(8,128)(2,1)S(1)} collective-permute-done((bf16[96,512]{1,0:T(8,128)(2,1)S(1)}, bf16[96,512]{1,0:T(8,128)(2,1)S(1)}, u32[]{:S(2)}, u32[]{:S(2)}) %collective-permute-start.9) | collective-permute-done | bytes 98336 | tf_op jit(solution)/shard_map/ppermute | solution.py:23
  70.4 1.0 %collective-permute-done.11.refs_1_ = bf16[96,512]{1,0:T(8,128)(2,1)S(1)} collective-permute-done((bf16[96,512]{1,0:T(8,128)(2,1)S(1)}, bf16[96,512]{1,0:T(8,128)(2,1)S(1)}, u32[]{:S(2)}, u32[]{:S(2)}) %collective-permute-start.11) | collective-permute-done | bytes 98336 | tf_op jit(solution)/shard_map/ppermute | solution.py:23
  71.4 4.3 %collective-permute-done.12.refs_2_ = bf16[96,512]{1,0:T(8,128)(2,1)S(1)} collective-permute-done((bf16[96,512]{1,0:T(8,128)(2,1)S(1)}, bf16[96,512]{1,0:T(8,128)(2,1)S(1)}, u32[]{:S(2)}, u32[]{:S(2)}) %collective-permute-start.12) | collective-permute-done | bytes 98336 | tf_op jit(solution)/shard_map/ppermute | solution.py:23
  75.7 1.9 %combine.1 = bf16[128,512]{1,0:T(8,128)(2,1)} custom-call(s32[2]{0:T(128)S(1)} %pad_add_fusion.scal, s32[128,2]{1,0:T(8,128)S(1)} %copy.13.routes_ref, f32[128,2]{1,0:T(8,128)S(1)} %copy.14.weights_ref, bf16[96,512]{1,0:T(8,128)(2,1)S(1)} %collective-permute-done.9.refs_0_, bf16[96,512]{1,0:T(8,128)(2,1)S(1)} %collective-permute-done.11.refs_1_, ...), custom_call_target="tpu_custom_call" | custom-call | tf_op jit(solution)/shard_map/combine/pallas_call | solution.py:104
  (42 shorter events, 5.5 us)
Async XLA Ops:
  0.6 39.3 %copy-start = (bf16[1,2048,896]{2,1,0:T(8,128)(2,1)S(1)}, bf16[1,2048,896]{2,1,0:T(8,128)(2,1)}, u32[]{:S(2)}) copy-start(bf16[1,2048,896]{2,1,0:T(8,128)(2,1)} %refs_0_.1) | copy-start | bytes 11010052
  0.7 1.2 %copy-start.5 = (bf16[128,2048]{1,0:T(8,128)(2,1)S(1)}, bf16[128,2048]{1,0:T(8,128)(2,1)}, u32[]{:S(2)}) copy-start(bf16[128,2048]{1,0:T(8,128)(2,1)} %x_ref.1) | copy-start | bytes 1572868
  1.9 0.7 copy-start.7
  2.6 0.7 copy-start.9
  5.1 6.4 %collective-permute-start.3 = (bf16[16,512]{1,0:T(8,128)(2,1)S(1)}, bf16[16,512]{1,0:T(8,128)(2,1)S(1)}, u32[]{:S(2)}, u32[]{:S(2)}) collective-permute-start(bf16[16,512]{1,0:T(8,128)(2,1)S(1)} %slice.57), channel_id=1, source_target_pairs={{0,4},{4,8},{8,12},{1,5},{5,9},{9,13},{2,6},{6,10},{10,14},{3,7},{... | collective-permute-start | bytes 49160 | tf_op jit(solution)/shard_map/ppermute | solution.py:18
  11.5 1.6 %copy-start.3 = (bf16[512,2048]{1,0:T(8,128)(2,1)S(1)}, bf16[512,2048]{1,0:T(8,128)(2,1)}, u32[]{:S(2)}) copy-start(bf16[512,2048]{1,0:T(8,128)(2,1)} %branch_hbm.1) | copy-start | bytes 6291460
  13.1 1.0 %copy-start.4 = (bf16[16,128,128]{2,1,0:T(8,128)(2,1)S(1)}, bf16[16,128,128]{2,1,0:T(8,128)(2,1)}, u32[]{:S(2)}) copy-start(bf16[16,128,128]{2,1,0:T(8,128)(2,1)} %group_hbm.1) | copy-start | bytes 1572868
  14.1 0.9 %copy-start.6 = (bf16[256,512]{1,0:T(8,128)(2,1)S(1)}, bf16[256,512]{1,0:T(8,128)(2,1)}, u32[]{:S(2)}) copy-start(bf16[256,512]{1,0:T(8,128)(2,1)} %x_hbm.1) | copy-start | bytes 786436
  15.1 0.7 copy-start.8
  18.0 2.0 %collective-permute-start.4 = (bf16[2,256,512]{2,1,0:T(8,128)(2,1)S(1)}, bf16[2,256,512]{2,1,0:T(8,128)(2,1)S(1)}, u32[]{:S(2)}, u32[]{:S(2)}) collective-permute-start(bf16[2,256,512]{2,1,0:T(8,128)(2,1)S(1)} %get-tuple-element.33), channel_id=1, source_target_pairs={{0,1},{1,0},{2,3},{3,2},{4,5},{5,4},{6,7},{7,6},{8,9},{9,8},{10,11... | collective-permute-start | bytes 1572872 | tf_op jit(solution)/shard_map/ppermute | solution.py:28
  20.0 8.7 %collective-permute-start.5 = (bf16[256,512]{1,0:T(8,128)(2,1)S(1)}, bf16[256,512]{1,0:T(8,128)(2,1)S(1)}, u32[]{:S(2)}, u32[]{:S(2)}) collective-permute-start(bf16[256,512]{1,0:T(8,128)(2,1)S(1)} %fusion.3), channel_id=1, source_target_pairs={{0,2},{1,3},{2,0},{3,1},{4,6},{5,7},{6,4},{7,5},{8,10},{9,11},{10,... | collective-permute-start | bytes 786440 | tf_op jit(solution)/shard_map/ppermute | solution.py:23
  21.6 17.5 %collective-permute-start = (bf16[96,1024]{1,0:T(8,128)(2,1)S(1)}, bf16[96,1024]{1,0:T(8,128)(2,1)S(1)}, u32[]{:S(2)}, u32[]{:S(2)}) collective-permute-start(bf16[96,1024]{1,0:T(8,128)(2,1)S(1)} %get-tuple-element.28), channel_id=1, source_target_pairs={{0,8},{4,12},{8,0},{12,4},{1,9},{5,13},{9,1},{13,5},{2,10},{6,14},... | collective-permute-start | bytes 589832 | tf_op jit(solution)/shard_map/ppermute | solution.py:23
  24.9 14.2 %collective-permute-start.1 = (bf16[96,1024]{1,0:T(8,128)(2,1)S(1)}, bf16[96,1024]{1,0:T(8,128)(2,1)S(1)}, u32[]{:S(2)}, u32[]{:S(2)}) collective-permute-start(bf16[96,1024]{1,0:T(8,128)(2,1)S(1)} %get-tuple-element.29), channel_id=1, source_target_pairs={{0,4},{4,8},{8,12},{12,0},{1,5},{5,9},{9,13},{13,1},{2,6},{6,10},{... | collective-permute-start | bytes 589832 | tf_op jit(solution)/shard_map/ppermute | solution.py:23
  26.4 13.4 %collective-permute-start.2 = (bf16[96,1024]{1,0:T(8,128)(2,1)S(1)}, bf16[96,1024]{1,0:T(8,128)(2,1)S(1)}, u32[]{:S(2)}, u32[]{:S(2)}) collective-permute-start(bf16[96,1024]{1,0:T(8,128)(2,1)S(1)} %get-tuple-element.30), channel_id=1, source_target_pairs={{0,12},{4,0},{8,4},{12,8},{1,13},{5,1},{9,5},{13,9},{2,14},{6,2},{... | collective-permute-start | bytes 589832 | tf_op jit(solution)/shard_map/ppermute | solution.py:23
  39.9 7.3 %collective-permute-start.6 = (bf16[384,1024]{1,0:T(8,128)(2,1)S(1)}, bf16[384,1024]{1,0:T(8,128)(2,1)S(1)}, u32[]{:S(2)}, u32[]{:S(2)}) collective-permute-start(bf16[384,1024]{1,0:T(8,128)(2,1)S(1)} %constant_dynamic-update-slice_fusion.mine_ref), channel_id=1, source_target_pairs={{0,1},{1,0},{2,3},{3,2},{4,5},{5,4},{6,7},{7,6},{8,9},{9,8},{10,11... | collective-permute-start | bytes 2359304 | tf_op jit(solution)/shard_map/ppermute | solution.py:28
  40.0 2.0 %copy-start.1 = (bf16[1,2048,896]{2,1,0:T(8,128)(2,1)S(1)}, bf16[1,2048,896]{2,1,0:T(8,128)(2,1)}, u32[]{:S(2)}) copy-start(bf16[1,2048,896]{2,1,0:T(8,128)(2,1)} %refs_1_.1) | copy-start | bytes 11010052
  42.0 2.0 %copy-start.2 = (bf16[1,896,2048]{2,1,0:T(8,128)(2,1)S(1)}, bf16[1,896,2048]{2,1,0:T(8,128)(2,1)}, u32[]{:S(2)}) copy-start(bf16[1,896,2048]{2,1,0:T(8,128)(2,1)} %refs_2_.1) | copy-start | bytes 11010052
  50.6 2.4 %collective-permute-start.7 = (bf16[2,384,512]{2,1,0:T(8,128)(2,1)S(1)}, bf16[2,384,512]{2,1,0:T(8,128)(2,1)S(1)}, u32[]{:S(2)}, u32[]{:S(2)}) collective-permute-start(bf16[2,384,512]{2,1,0:T(8,128)(2,1)S(1)} %get-tuple-element.45), channel_id=1, source_target_pairs={{0,1},{1,0},{2,3},{3,2},{4,5},{5,4},{6,7},{7,6},{8,9},{9,8},{10,11... | collective-permute-start | bytes 2359304 | tf_op jit(solution)/shard_map/ppermute | solution.py:28
  51.1 17.4 %copy-start.10 = (s32[128,2]{0,1:T(2,128)S(1)}, s32[128,2]{0,1:T(2,128)}, u32[]{:S(2)}) copy-start(s32[128,2]{0,1:T(2,128)} %param.17) | copy-start | bytes 3076
  51.1 17.5 %copy-start.11 = (f32[128,2]{0,1:T(2,128)S(1)}, f32[128,2]{0,1:T(2,128)}, u32[]{:S(2)}) copy-start(f32[128,2]{0,1:T(2,128)} %param.18) | copy-start | bytes 3076
  53.1 5.7 %collective-permute-start.13 = (bf16[96,512]{1,0:T(8,128)(2,1)S(1)}, bf16[96,512]{1,0:T(8,128)(2,1)S(1)}, u32[]{:S(2)}, u32[]{:S(2)}) collective-permute-start(bf16[96,512]{1,0:T(8,128)(2,1)S(1)} %get-tuple-element.48), channel_id=1, source_target_pairs={{0,2},{1,3},{2,0},{3,1},{4,6},{5,7},{6,4},{7,5},{8,10},{9,11},{10,... | collective-permute-start | bytes 294920 | tf_op jit(solution)/shard_map/ppermute | solution.py:23
  53.7 7.2 %collective-permute-start.8 = (bf16[96,512]{1,0:T(8,128)(2,1)S(1)}, bf16[96,512]{1,0:T(8,128)(2,1)S(1)}, u32[]{:S(2)}, u32[]{:S(2)}) collective-permute-start(bf16[96,512]{1,0:T(8,128)(2,1)S(1)} %get-tuple-element.49), channel_id=1, source_target_pairs={{0,2},{1,3},{2,0},{3,1},{4,6},{5,7},{6,4},{7,5},{8,10},{9,11},{10,... | collective-permute-start | bytes 294920 | tf_op jit(solution)/shard_map/ppermute | solution.py:23
  55.2 11.1 %collective-permute-start.10 = (bf16[192,512]{1,0:T(8,128)(2,1)S(1)}, bf16[192,512]{1,0:T(8,128)(2,1)S(1)}, u32[]{:S(2)}, u32[]{:S(2)}) collective-permute-start(bf16[192,512]{1,0:T(8,128)(2,1)S(1)} %fusion.5), channel_id=1, source_target_pairs={{0,2},{1,3},{2,0},{3,1},{4,6},{5,7},{6,4},{7,5},{8,10},{9,11},{10,... | collective-permute-start | bytes 589832 | tf_op jit(solution)/shard_map/ppermute | solution.py:23
  61.0 9.4 %collective-permute-start.9 = (bf16[96,512]{1,0:T(8,128)(2,1)S(1)}, bf16[96,512]{1,0:T(8,128)(2,1)S(1)}, u32[]{:S(2)}, u32[]{:S(2)}) collective-permute-start(bf16[96,512]{1,0:T(8,128)(2,1)S(1)} %get-tuple-element.47), channel_id=1, source_target_pairs={{0,8},{4,12},{8,0},{12,4},{1,9},{5,13},{9,1},{13,5},{2,10},{6,14},... | collective-permute-start | bytes 294920 | tf_op jit(solution)/shard_map/ppermute | solution.py:23
  66.4 5.0 %collective-permute-start.11 = (bf16[96,512]{1,0:T(8,128)(2,1)S(1)}, bf16[96,512]{1,0:T(8,128)(2,1)S(1)}, u32[]{:S(2)}, u32[]{:S(2)}) collective-permute-start(bf16[96,512]{1,0:T(8,128)(2,1)S(1)} %get-tuple-element.51), channel_id=1, source_target_pairs={{0,12},{4,0},{8,4},{12,8},{1,13},{5,1},{9,5},{13,9},{2,14},{6,2},{... | collective-permute-start | bytes 294920 | tf_op jit(solution)/shard_map/ppermute | solution.py:23
  66.9 8.8 %collective-permute-start.12 = (bf16[96,512]{1,0:T(8,128)(2,1)S(1)}, bf16[96,512]{1,0:T(8,128)(2,1)S(1)}, u32[]{:S(2)}, u32[]{:S(2)}) collective-permute-start(bf16[96,512]{1,0:T(8,128)(2,1)S(1)} %get-tuple-element.50), channel_id=1, source_target_pairs={{0,4},{4,8},{8,12},{12,0},{1,5},{5,9},{9,13},{13,1},{2,6},{6,10},{... | collective-permute-start | bytes 294920 | tf_op jit(solution)/shard_map/ppermute | solution.py:23
where the time goes:
time: 78.1 us; the launch traced here: 77.6 us
  waiting for transfers between devices  26.1 us (33%)
  starting transfers between devices  24.4 us (31%)
  Pallas kernels  13.2 us (17%)
  local copies, waits for them, and re-layouts  11.9 us (15%)
  other arithmetic  1.19 us (2%)
  between operations  0.81 us (1%)
    ppermute x10, waiting for transfers between devices, rotated(): lax.ppermute(block, axis, [(i, (i + distance) % count) for i in range(cou...  22.4 us
    ppermute x10, starting transfers between devices, rotated(): lax.ppermute(block, axis, [(i, (i + distance) % count) for i in range(cou...  18.8 us
    unnamed x29, local copies, waits for them, and re-layouts  11.2 us
    pallas_call x3, Pallas kernels, whole_call(): pl.pallas_call(body, in_specs=[pl.BlockSpec(memory_space=pltpu.SMEM)] + [...  7.26 us
    ppermute x1, starting transfers between devices, shifted(): return lax.ppermute(block, axis, route)  4.94 us
    ppermute x3, waiting for transfers between devices, paired(): return lax.ppermute(block, 'tp', [(i, i ^ 1) for i in range(count)])  2.26 us
    pallas_call x1, Pallas kernels, mixer(): pl.pallas_call(body, in_specs=[pl.BlockSpec(memory_space=pltpu.SMEM), hbm...  2.17 us
    pallas_call x1, Pallas kernels, combine(): pl.pallas_call(body, in_specs=[pl.BlockSpec(memory_space=pltpu.SMEM)] + [...  1.91 us
  transfers between devices with their start and end apart: 14, of which 10 were waited for; matrix products, arithmetic and copies ran while one was open for 2% of the time, Pallas kernels for 6%

commit v1 on v0

--- a/solution.py
+++ b/solution.py
@@ -10,12 +10,6 @@
 halo = 16
 f32, bf16 = jnp.float32, jnp.bfloat16
 params = pltpu.CompilerParams(vmem_limit_bytes=24 * 2**20)
-
-
-def shifted(block, axis, distance):
-    devices = range(lax.axis_size(axis))
-    route = [(i - distance, i) for i in devices if i - distance in devices]
-    return lax.ppermute(block, axis, route)
 
 
 def rotated(block, axis, distance):
@@ -83,33 +77,39 @@
     )(scalars, exp_input, norm_gain.reshape(1, width), routes.T)
 
 
-def combine(scalars, routes, route_weights, chunks, order):
+def picks_of(scalars, routes, capacity, order):
     tokens, top = routes.shape
-    capacity, columns = chunks[0].shape
     experts = len(order)
 
-    def body(scal, routes_ref, weights_ref, *refs):
-        out = refs[-1]
+    def body(scal, routes_ref, *outs):
         places, _ = ranks_of(routes_ref[...], scal[1], experts)
         slots = lax.broadcasted_iota(jnp.int32, (tokens, capacity), 1).astype(f32)
+        for out, e in zip(outs, order):
+            for k in range(top):
+                out[k * tokens : (k + 1) * tokens] = jnp.where(
+                    places[k][:, e : e + 1] == slots, 1.0, 0.0
+                ).astype(bf16)
+
+    shape = jax.ShapeDtypeStruct((top * tokens, capacity), bf16)
+    return whole_call(body, [shape] * experts, scalars, routes)
+
+
+def combine(scalars, picks, route_weights, chunks):
+    tokens, top = route_weights.shape
+    columns = chunks[0].shape[1]
+    count = len(chunks)
+
+    def body(scal, weights_ref, *refs):
+        chosen = jnp.zeros((top * tokens, columns), f32)
+        for pick, chunk in zip(refs[:count], refs[count:-1]):
+            chosen = chosen + jnp.dot(pick[...], chunk[...], preferred_element_type=f32)
         total = jnp.zeros((tokens, columns), f32)
         for k in range(top):
-            chosen = jnp.zeros((tokens, columns), f32)
-            for ref, e in zip(refs, order):
-                pick = jnp.where(places[k][:, e : e + 1] == slots, 1.0, 0.0).astype(bf16)
-                chosen = chosen + jnp.dot(pick, ref[...], preferred_element_type=f32)
-            total = total + chosen * weights_ref[:, k : k + 1]
-        out[...] = total.astype(bf16)
-
-    return pl.pallas_call(
-        body,
-        in_specs=[pl.BlockSpec(memory_space=pltpu.SMEM)]
-        + [pl.BlockSpec(memory_space=pltpu.VMEM)] * (2 + experts),
-        out_specs=pl.BlockSpec(memory_space=pltpu.VMEM),
-        out_shape=jax.ShapeDtypeStruct((tokens, columns), bf16),
-        name="combine",
-        compiler_params=params,
-    )(scalars, routes, route_weights, *chunks)
+            total = total + chosen[k * tokens : (k + 1) * tokens] * weights_ref[:, k : k + 1]
+        refs[-1][...] = total.astype(bf16)
+
+    shape = jax.ShapeDtypeStruct((tokens, columns), bf16)
+    return whole_call(body, [shape], scalars, route_weights, *picks, *chunks)[0]
 
 
 def column_block(step, rank, chips):
@@ -142,9 +142,8 @@
         place = scal[1] * rows + lax.broadcasted_iota(jnp.int32, (rows, group_width), 0)
         for g in range(group_count):
             cut = slice(g * group_width, (g + 1) * group_width)
-            extended = jnp.concatenate(
-                [before_ref[:, cut].astype(f32), x_ref[:, cut].astype(f32)], axis=0
-            )
+            earlier = jnp.where(scal[1] > 0, before_ref[:, cut].astype(f32), 0.0)
+            extended = jnp.concatenate([earlier, x_ref[:, cut].astype(f32)], axis=0)
             level = lax.rem(scal[0] * group_count + g, len(windows))
             sums = extended
             chosen = jnp.zeros_like(extended)
@@ -279,7 +278,9 @@
 def reduced(got, keep, cuts):
     chips = keep.shape[0]
     pieces = []
-    for start, stop in cuts:
+    for index, (start, stop) in enumerate(cuts):
+        if index:
+            got, keep = lax.optimization_barrier((got, keep))
         part = [
             (keep[r, start:stop].astype(f32) + got[r, start:stop].astype(f32)).astype(bf16)
             for r in range(chips)
@@ -316,18 +317,18 @@
     arrivals = []
     for block, k in zip(outgoing[:-1], order):
         arrivals.append(rotated(block, "ep", k))
-    before = shifted(late_mix[rows_mix - halo :], "ep", 1)
+    before = rotated(late_mix[rows_mix - halo :], "ep", 1)
     give, keep = mixer(scalars, mix_input, before, group_weight, pool_gain, branch_weight, members)
     got = paired(give)
     (mix_out,) = reduced(got, keep, [(0, rows_mix)])
     gate_weight, up_weight, down_weight = load(gate_weight, up_weight, down_weight)
-    *arrivals, mix_out = lax.optimization_barrier((*arrivals, mix_out))
     mine = jnp.concatenate([*arrivals, outgoing[-1]], axis=0)
     theirs = paired(mine)
     gate, up = enter(scalars, mine, gate_weight, up_weight)
     hidden, give = middle(scalars, theirs, gate_weight, up_weight, gate, up, down_weight, members)
     got = paired(give)
     keep = leave(scalars, hidden, down_weight, members)
+    picks = picks_of(scalars, routes, capacity, order)
     groups = [order[:1], order[1:-1], order[-1:]]
     cuts, at = [], 0
     for group in groups:
@@ -338,7 +339,7 @@
         for j, k in enumerate(group):
             part = piece[j * capacity : (j + 1) * capacity]
             chunks.append(rotated(part, "ep", -k) if k else part)
-    exp_out = combine(scalars, routes, route_weights, chunks, order)
+    exp_out = combine(scalars, picks, route_weights, chunks)
     return (mix_out, exp_out)
 
 

time: 78.1 us -> 84.4 us (1.081)
  waiting for transfers between devices: 26.1 us -> 29.2 us
  local copies, waits for them, and re-layouts: 11.9 us -> 14.7 us
  starting transfers between devices: 24.4 us -> 23 us
  other arithmetic: 1.19 us -> 2.26 us
    ppermute x10 -> x11, waiting for transfers between devices: 22.4 us -> 29.2 us  [rotated(): lax.ppermute(block, axis, [(i, (i + distance) % count) for i in range(cou...]
    ppermute x1 -> x0, starting transfers between devices: 4.94 us -> none  [shifted(): return lax.ppermute(block, axis, route)]
    ppermute x10 -> x11, starting transfers between devices: 18.8 us -> 22.3 us  [rotated(): lax.ppermute(block, axis, [(i, (i + distance) % count) for i in range(cou...]
    unnamed x29 -> x35, local copies, waits for them, and re-layouts: 11.2 us -> 14 us
    pallas_call x3 -> x5, Pallas kernels: 7.26 us -> 9.83 us  [whole_call(): pl.pallas_call(body, in_specs=[pl.BlockSpec(memory_space=pltpu.SMEM)] + [...]
    ppermute x3, waiting for transfers between devices: 2.26 us -> 0.01 us  [paired(): return lax.ppermute(block, 'tp', [(i, i ^ 1) for i in range(count)])]
    pallas_call x1 -> x0, Pallas kernels: 1.91 us -> none  [combine(): pl.pallas_call(body, in_specs=[pl.BlockSpec(memory_space=pltpu.SMEM)] + [...]
    ppermute x1 -> x0, waiting for transfers between devices: 1.43 us -> none  [shifted(): return lax.ppermute(block, axis, route)]
  transfers between devices with their start and end apart: 14 -> 14, of which waited for: 10 -> 8; matrix products, arithmetic and copies ran while one was open for 2% -> 4% of each run, Pallas kernels for 6% -> 13%
where the time goes in v1:
time: 84.4 us; the launch traced here: 83.9 us
  waiting for transfers between devices  29.2 us (35%)
  starting transfers between devices  23 us (27%)
  local copies, waits for them, and re-layouts  14.7 us (17%)
  Pallas kernels  13.9 us (16%)
  other arithmetic  2.26 us (3%)
  between operations  0.88 us (1%)
    ppermute x11, waiting for transfers between devices, rotated(): lax.ppermute(block, axis, [(i, (i + distance) % count) for i in range(cou...  29.2 us
    ppermute x11, starting transfers between devices, rotated(): lax.ppermute(block, axis, [(i, (i + distance) % count) for i in range(cou...  22.3 us
    unnamed x35, local copies, waits for them, and re-layouts  14 us
    pallas_call x5, Pallas kernels, whole_call(): pl.pallas_call(body, in_specs=[pl.BlockSpec(memory_space=pltpu.SMEM)] + [...  9.83 us
    pallas_call x1, Pallas kernels, mixer(): pl.pallas_call(body, in_specs=[pl.BlockSpec(memory_space=pltpu.SMEM), hbm...  2.19 us
    convert_element_type x4, other arithmetic, reduced(): pieces.append(total.astype(bf16))  2.01 us
  transfers between devices with their start and end apart: 14, of which 8 were waited for; matrix products, arithmetic and copies ran while one was open for 4% of the time, Pallas kernels for 13%

profile of v1, /device:TPU:0, one launch (start us, length us, event | category | flops | bytes accessed | tf_op | source)
XLA Modules:
  0.0 83.9 jit_solution(10264431764778934521)
XLA Ops:
  0.7 1.2 %copy-done.7 = bf16[128,2048]{1,0:T(8,128)(2,1)S(1)} copy-done((bf16[128,2048]{1,0:T(8,128)(2,1)S(1)}, bf16[128,2048]{1,0:T(8,128)(2,1)}, u32[]{:S(2)}) %copy-start.7) | copy-done | bytes 524312
  3.3 1.1 %prepare.1 = (bf16[96,1024]{1,0:T(8,128)(2,1)S(1)}, bf16[96,1024]{1,0:T(8,128)(2,1)S(1)}, bf16[96,1024]{1,0:T(8,128)(2,1)S(1)}, bf16[96,1024]{1,0:T(8,128)(2,1)S(1)}) custom-call(s32[2]{0:T(128)S(1)} %pad_add_fusion.scal, bf16[128,2048]{1,0:T(8,128)(2,1)S(1)} %copy-done.7, f32[1,2048]{1,0:T(1,128)S(1)} %bitcast.33, s32[2,128]{1,0:T(2,128)S(1)} %bitcast.35), custom_call_target="tpu_custom_call" | custom-call | tf_op jit(solution)/shard_map/prepare/pallas_call | solution.py:65
  4.4 4.1 %collective-permute-start.3 = (bf16[96,1024]{1,0:T(8,128)(2,1)S(1)}, bf16[96,1024]{1,0:T(8,128)(2,1)S(1)}, u32[]{:S(2)}, u32[]{:S(2)}) collective-permute-start(bf16[96,1024]{1,0:T(8,128)(2,1)S(1)} %get-tuple-element.39), channel_id=1, source_target_pairs={{0,8},{4,12},{8,0},{12,4},{1,9},{5,13},{9,1},{13,5},{2,10},{6,14},... | collective-permute-start | bytes 589832 | tf_op jit(solution)/shard_map/ppermute | solution.py:17
  8.5 1.6 %collective-permute-start.4 = (bf16[96,1024]{1,0:T(8,128)(2,1)S(1)}, bf16[96,1024]{1,0:T(8,128)(2,1)S(1)}, u32[]{:S(2)}, u32[]{:S(2)}) collective-permute-start(bf16[96,1024]{1,0:T(8,128)(2,1)S(1)} %get-tuple-element.40), channel_id=1, source_target_pairs={{0,4},{4,8},{8,12},{12,0},{1,5},{5,9},{9,13},{13,1},{2,6},{6,10},{... | collective-permute-start | bytes 589832 | tf_op jit(solution)/shard_map/ppermute | solution.py:17
  10.1 2.2 %collective-permute-start.5 = (bf16[96,1024]{1,0:T(8,128)(2,1)S(1)}, bf16[96,1024]{1,0:T(8,128)(2,1)S(1)}, u32[]{:S(2)}, u32[]{:S(2)}) collective-permute-start(bf16[96,1024]{1,0:T(8,128)(2,1)S(1)} %get-tuple-element.41), channel_id=1, source_target_pairs={{0,12},{4,0},{8,4},{12,8},{1,13},{5,1},{9,5},{13,9},{2,14},{6,2},{... | collective-permute-start | bytes 589832 | tf_op jit(solution)/shard_map/ppermute | solution.py:17
  12.4 10.4 %collective-permute-done.3 = bf16[96,1024]{1,0:T(8,128)(2,1)S(1)} collective-permute-done((bf16[96,1024]{1,0:T(8,128)(2,1)S(1)}, bf16[96,1024]{1,0:T(8,128)(2,1)S(1)}, u32[]{:S(2)}, u32[]{:S(2)}) %collective-permute-start.3) | collective-permute-done | bytes 196640 | tf_op jit(solution)/shard_map/ppermute | solution.py:17
  24.3 3.4 %collective-permute-start = (bf16[16,512]{1,0:T(8,128)(2,1)S(1)}, bf16[16,512]{1,0:T(8,128)(2,1)S(1)}, u32[]{:S(2)}, u32[]{:S(2)}) collective-permute-start(bf16[16,512]{1,0:T(8,128)(2,1)S(1)} %slice.57), channel_id=1, source_target_pairs={{0,4},{4,8},{8,12},{12,0},{1,5},{5,9},{9,13},{13,1},{2,6},{6,10},{... | collective-permute-start | bytes 49160 | tf_op jit(solution)/shard_map/ppermute | solution.py:17
  27.7 2.2 %collective-permute-done.before_ref = bf16[16,512]{1,0:T(8,128)(2,1)S(1)} collective-permute-done((bf16[16,512]{1,0:T(8,128)(2,1)S(1)}, bf16[16,512]{1,0:T(8,128)(2,1)S(1)}, u32[]{:S(2)}, u32[]{:S(2)}) %collective-permute-start) | collective-permute-done | bytes 16416 | tf_op jit(solution)/shard_map/ppermute | solution.py:17
  29.8 1.6 %copy-done.5 = bf16[512,2048]{1,0:T(8,128)(2,1)S(1)} copy-done((bf16[512,2048]{1,0:T(8,128)(2,1)S(1)}, bf16[512,2048]{1,0:T(8,128)(2,1)}, u32[]{:S(2)}) %copy-start.5) | copy-done | bytes 2097176
  31.4 1.0 %copy-done.6 = bf16[16,128,128]{2,1,0:T(8,128)(2,1)S(1)} copy-done((bf16[16,128,128]{2,1,0:T(8,128)(2,1)S(1)}, bf16[16,128,128]{2,1,0:T(8,128)(2,1)}, u32[]{:S(2)}) %copy-start.6) | copy-done | bytes 524312
  32.5 0.9 %copy-done.8 = bf16[256,512]{1,0:T(8,128)(2,1)S(1)} copy-done((bf16[256,512]{1,0:T(8,128)(2,1)S(1)}, bf16[256,512]{1,0:T(8,128)(2,1)}, u32[]{:S(2)}) %copy-start.8) | copy-done | bytes 262168
  34.1 2.2 %mixer.1 = (bf16[2,256,512]{2,1,0:T(8,128)(2,1)S(1)}, bf16[2,256,512]{2,1,0:T(8,128)(2,1)S(1)}) custom-call(s32[2]{0:T(128)S(1)} %pad_add_fusion.scal, bf16[256,512]{1,0:T(8,128)(2,1)S(1)} %copy-done.8, bf16[16,512]{1,0:T(8,128)(2,1)S(1)} %collective-permute-done.before_ref, bf16[16,128,128]{2,1,0:T(8,128)(2,1)S(1)} %copy-done.6, f32[1,2048]{1,0:T(1,128)S(1)} %bitcast.34, ...), custom_call_target="tpu_custom_call" | custom-call | tf_op jit(solution)/shard_map/mixer/pallas_call | solution.py:172
  36.4 2.0 %copy-done.3 = bf16[1,2048,896]{2,1,0:T(8,128)(2,1)S(1)} copy-done((bf16[1,2048,896]{2,1,0:T(8,128)(2,1)S(1)}, bf16[1,2048,896]{2,1,0:T(8,128)(2,1)}, u32[]{:S(2)}) %copy-start.3) | copy-done | bytes 3670040
  38.4 2.0 %copy-done.4 = bf16[1,896,2048]{2,1,0:T(8,128)(2,1)S(1)} copy-done((bf16[1,896,2048]{2,1,0:T(8,128)(2,1)S(1)}, bf16[1,896,2048]{2,1,0:T(8,128)(2,1)}, u32[]{:S(2)}) %copy-start.4) | copy-done | bytes 3670040
  40.5 0.8 load.1
  41.3 2.3 %shard_map.123 = (f32[384,896]{1,0:T(8,128)S(1)}, f32[384,896]{1,0:T(8,128)S(1)}) custom-call(s32[2]{0:T(128)S(1)} %pad_add_fusion.scal, bf16[384,1024]{1,0:T(8,128)(2,1)S(1)} %constant_dynamic-update-slice_fusion.mine_ref, bf16[1,2048,896]{2,1,0:T(8,128)(2,1)S(1)} %get-tuple-element.43.gate_ref, bf16[1,2048,896]{2,1,0:T(8,128)(2,1)S(1)} %get-tuple-element.44.up_ref), custom_call_target="tpu_custom_call" | custom-call | tf_op jit(solution)/shard_map/pallas_call | solution.py:215
  43.7 3.4 %shard_map.124 = (bf16[384,896]{1,0:T(8,128)(2,1)S(1)}, bf16[2,384,512]{2,1,0:T(8,128)(2,1)S(1)}) custom-call(s32[2]{0:T(128)S(1)} %pad_add_fusion.scal, bf16[384,1024]{1,0:T(8,128)(2,1)S(1)} %collective-permute-done.6.theirs_ref, bf16[1,2048,896]{2,1,0:T(8,128)(2,1)S(1)} %get-tuple-element.43.gate_ref, bf16[1,2048,896]{2,1,0:T(8,128)(2,1)S(1)} %get-tuple-element.44.up_ref, ...), custom_call_target="tpu_custom_call" | custom-call | tf_op jit(solution)/shard_map/pallas_call | solution.py:215
  48.4 1.5 %collective-permute-start.2 = (bf16[256,512]{1,0:T(8,128)(2,1)S(1)}, bf16[256,512]{1,0:T(8,128)(2,1)}, u32[]{:S(2)}, u32[]{:S(2)}) collective-permute-start(bf16[256,512]{1,0:T(8,128)(2,1)S(1)} %fusion.3), channel_id=1, source_target_pairs={{0,2},{1,3},{2,0},{3,1},{4,6},{5,7},{6,4},{7,5},{8,10},{9,11},{10,... | collective-permute-start | bytes 786440 | tf_op jit(solution)/shard_map/ppermute | solution.py:17
  50.0 1.0 %shard_map.122 = (bf16[256,96]{1,0:T(8,128)(2,1)S(1)}, bf16[256,96]{1,0:T(8,128)(2,1)S(1)}, bf16[256,96]{1,0:T(8,128)(2,1)S(1)}, bf16[256,96]{1,0:T(8,128)(2,1)S(1)}) custom-call(s32[2]{0:T(128)S(1)} %pad_add_fusion.scal, s32[128,2]{1,0:T(8,128)S(1)} %copy.13.routes_ref), custom_call_target="tpu_custom_call" | custom-call | tf_op jit(solution)/shard_map/pallas_call | solution.py:215
  51.1 5.6 %collective-permute-done.2 = bf16[256,512]{1,0:T(8,128)(2,1)} collective-permute-done((bf16[256,512]{1,0:T(8,128)(2,1)S(1)}, bf16[256,512]{1,0:T(8,128)(2,1)}, u32[]{:S(2)}, u32[]{:S(2)}) %collective-permute-start.2) | collective-permute-done | bytes 262176 | tf_op jit(solution)/shard_map/ppermute | solution.py:17
  56.7 1.9 %fusion = bf16[256,512]{1,0:T(8,128)(2,1)} fusion(bf16[256,512]{1,0:T(8,128)(2,1)} %collective-permute-done.2, bf16[2,256,512]{2,1,0:T(8,128)(2,1)} %copy-done.13, bf16[2,256,512]{2,1,0:T(8,128)(2,1)S(1)} %get-tuple-element.33), kind=kLoop, calls=%fused_computation.1 | loop fusion | flops 1048576 | bytes 1048576 | tf_op jit(solution)/shard_map/convert_element_type | solution.py:292
  58.6 2.0 %copy-done.1 = bf16[1,896,2048]{2,1,0:T(8,128)(2,1)S(1)} copy-done((bf16[1,896,2048]{2,1,0:T(8,128)(2,1)S(1)}, bf16[1,896,2048]{2,1,0:T(8,128)(2,1)}, u32[]{:S(2)}) %copy-start.1) | copy-done | bytes 3670040
  60.6 1.5 %shard_map.125 = bf16[2,384,512]{2,1,0:T(8,128)(2,1)S(1)} custom-call(s32[2]{0:T(128)S(1)} %pad_add_fusion.scal, bf16[384,896]{1,0:T(8,128)(2,1)S(1)} %get-tuple-element.48.hidden_ref, bf16[1,896,2048]{2,1,0:T(8,128)(2,1)S(1)} %copy-done.1), custom_call_target="tpu_custom_call" | custom-call | tf_op jit(solution)/shard_map/pallas_call | solution.py:215
  62.2 1.6 %collective-permute-start.13 = (bf16[96,512]{1,0:T(8,128)(2,1)S(1)}, bf16[96,512]{1,0:T(8,128)(2,1)S(1)}, u32[]{:S(2)}, u32[]{:S(2)}) collective-permute-start(bf16[96,512]{1,0:T(8,128)(2,1)S(1)} %fusion.11), channel_id=1, source_target_pairs={{0,2},{1,3},{2,0},{3,1},{4,6},{5,7},{6,4},{7,5},{8,10},{9,11},{10,... | collective-permute-start | bytes 294920 | tf_op jit(solution)/shard_map/ppermute | solution.py:17
  64.5 1.6 %collective-permute-start.10 = (bf16[192,512]{1,0:T(8,128)(2,1)S(1)}, bf16[192,512]{1,0:T(8,128)(2,1)S(1)}, u32[]{:S(2)}, u32[]{:S(2)}) collective-permute-start(bf16[192,512]{1,0:T(8,128)(2,1)S(1)} %fusion.5), channel_id=1, source_target_pairs={{0,2},{1,3},{2,0},{3,1},{4,6},{5,7},{6,4},{7,5},{8,10},{9,11},{10,... | collective-permute-start | bytes 589832 | tf_op jit(solution)/shard_map/ppermute | solution.py:17
  66.1 4.0 %collective-permute-done.8 = bf16[96,512]{1,0:T(8,128)(2,1)S(1)} collective-permute-done((bf16[96,512]{1,0:T(8,128)(2,1)S(1)}, bf16[96,512]{1,0:T(8,128)(2,1)S(1)}, u32[]{:S(2)}, u32[]{:S(2)}) %collective-permute-start.8) | collective-permute-done | bytes 98336 | tf_op jit(solution)/shard_map/ppermute | solution.py:17
  70.1 3.6 %collective-permute-start.9 = (bf16[96,512]{1,0:T(8,128)(2,1)S(1)}, bf16[96,512]{1,0:T(8,128)(2,1)S(1)}, u32[]{:S(2)}, u32[]{:S(2)}) collective-permute-start(bf16[96,512]{1,0:T(8,128)(2,1)S(1)} %fusion.7), channel_id=1, source_target_pairs={{0,8},{4,12},{8,0},{12,4},{1,9},{5,13},{9,1},{13,5},{2,10},{6,14},... | collective-permute-start | bytes 294920 | tf_op jit(solution)/shard_map/ppermute | solution.py:17
  73.8 2.1 %collective-permute-start.11 = (bf16[96,512]{1,0:T(8,128)(2,1)S(1)}, bf16[96,512]{1,0:T(8,128)(2,1)S(1)}, u32[]{:S(2)}, u32[]{:S(2)}) collective-permute-start(bf16[96,512]{1,0:T(8,128)(2,1)S(1)} %get-tuple-element.55), channel_id=1, source_target_pairs={{0,12},{4,0},{8,4},{12,8},{1,13},{5,1},{9,5},{13,9},{2,14},{6,2},{... | collective-permute-start | bytes 294920 | tf_op jit(solution)/shard_map/ppermute | solution.py:17
  75.9 1.8 %collective-permute-done.9.refs_4_ = bf16[96,512]{1,0:T(8,128)(2,1)S(1)} collective-permute-done((bf16[96,512]{1,0:T(8,128)(2,1)S(1)}, bf16[96,512]{1,0:T(8,128)(2,1)S(1)}, u32[]{:S(2)}, u32[]{:S(2)}) %collective-permute-start.9) | collective-permute-done | bytes 98336 | tf_op jit(solution)/shard_map/ppermute | solution.py:17
  77.7 1.1 %collective-permute-done.11.refs_5_ = bf16[96,512]{1,0:T(8,128)(2,1)S(1)} collective-permute-done((bf16[96,512]{1,0:T(8,128)(2,1)S(1)}, bf16[96,512]{1,0:T(8,128)(2,1)S(1)}, u32[]{:S(2)}, u32[]{:S(2)}) %collective-permute-start.11) | collective-permute-done | bytes 98336 | tf_op jit(solution)/shard_map/ppermute | solution.py:17
  78.8 3.4 %collective-permute-done.12.refs_6_ = bf16[96,512]{1,0:T(8,128)(2,1)S(1)} collective-permute-done((bf16[96,512]{1,0:T(8,128)(2,1)S(1)}, bf16[96,512]{1,0:T(8,128)(2,1)S(1)}, u32[]{:S(2)}, u32[]{:S(2)}) %collective-permute-start.12) | collective-permute-done | bytes 98336 | tf_op jit(solution)/shard_map/ppermute | solution.py:17
  82.3 1.6 %shard_map.126 = bf16[128,512]{1,0:T(8,128)(2,1)} custom-call(s32[2]{0:T(128)S(1)} %pad_add_fusion.scal, f32[128,2]{1,0:T(8,128)S(1)} %copy.14.weights_ref, bf16[256,96]{1,0:T(8,128)(2,1)S(1)} %get-tuple-element.35.refs_0_, bf16[256,96]{1,0:T(8,128)(2,1)S(1)} %get-tuple-element.36.refs_1_, bf16[256,96]{1,0:T(8,128)(2,1)S(1)} %get-tuple-element.37.refs_2_, ...), custom_call_target="tpu_custom_call" | custom-call | tf_op jit(solution)/shard_map/pallas_call | solution.py:215
  (51 shorter events, 6.1 us)
Async XLA Ops:
  0.6 35.8 %copy-start.2 = (bf16[1,2048,896]{2,1,0:T(8,128)(2,1)S(1)}, bf16[1,2048,896]{2,1,0:T(8,128)(2,1)}, u32[]{:S(2)}) copy-start(bf16[1,2048,896]{2,1,0:T(8,128)(2,1)} %refs_0_.1) | copy-start | bytes 11010052
  0.7 1.2 %copy-start.7 = (bf16[128,2048]{1,0:T(8,128)(2,1)S(1)}, bf16[128,2048]{1,0:T(8,128)(2,1)}, u32[]{:S(2)}) copy-start(bf16[128,2048]{1,0:T(8,128)(2,1)} %x_ref.1) | copy-start | bytes 1572868
  1.9 0.7 copy-start.9
  2.6 0.7 copy-start.11
  4.4 18.4 %collective-permute-start.3 = (bf16[96,1024]{1,0:T(8,128)(2,1)S(1)}, bf16[96,1024]{1,0:T(8,128)(2,1)S(1)}, u32[]{:S(2)}, u32[]{:S(2)}) collective-permute-start(bf16[96,1024]{1,0:T(8,128)(2,1)S(1)} %get-tuple-element.39), channel_id=1, source_target_pairs={{0,8},{4,12},{8,0},{12,4},{1,9},{5,13},{9,1},{13,5},{2,10},{6,14},... | collective-permute-start | bytes 589832 | tf_op jit(solution)/shard_map/ppermute | solution.py:17
  8.5 14.2 %collective-permute-start.4 = (bf16[96,1024]{1,0:T(8,128)(2,1)S(1)}, bf16[96,1024]{1,0:T(8,128)(2,1)S(1)}, u32[]{:S(2)}, u32[]{:S(2)}) collective-permute-start(bf16[96,1024]{1,0:T(8,128)(2,1)S(1)} %get-tuple-element.40), channel_id=1, source_target_pairs={{0,4},{4,8},{8,12},{12,0},{1,5},{5,9},{9,13},{13,1},{2,6},{6,10},{... | collective-permute-start | bytes 589832 | tf_op jit(solution)/shard_map/ppermute | solution.py:17
  10.1 13.3 %collective-permute-start.5 = (bf16[96,1024]{1,0:T(8,128)(2,1)S(1)}, bf16[96,1024]{1,0:T(8,128)(2,1)S(1)}, u32[]{:S(2)}, u32[]{:S(2)}) collective-permute-start(bf16[96,1024]{1,0:T(8,128)(2,1)S(1)} %get-tuple-element.41), channel_id=1, source_target_pairs={{0,12},{4,0},{8,4},{12,8},{1,13},{5,1},{9,5},{13,9},{2,14},{6,2},{... | collective-permute-start | bytes 589832 | tf_op jit(solution)/shard_map/ppermute | solution.py:17
  23.5 20.1 %collective-permute-start.6 = (bf16[384,1024]{1,0:T(8,128)(2,1)S(1)}, bf16[384,1024]{1,0:T(8,128)(2,1)S(1)}, u32[]{:S(2)}, u32[]{:S(2)}) collective-permute-start(bf16[384,1024]{1,0:T(8,128)(2,1)S(1)} %constant_dynamic-update-slice_fusion.mine_ref), channel_id=1, source_target_pairs={{0,1},{1,0},{2,3},{3,2},{4,5},{5,4},{6,7},{7,6},{8,9},{9,8},{10,11... | collective-permute-start | bytes 2359304 | tf_op jit(solution)/shard_map/ppermute | solution.py:22
  24.3 5.5 %collective-permute-start = (bf16[16,512]{1,0:T(8,128)(2,1)S(1)}, bf16[16,512]{1,0:T(8,128)(2,1)S(1)}, u32[]{:S(2)}, u32[]{:S(2)}) collective-permute-start(bf16[16,512]{1,0:T(8,128)(2,1)S(1)} %slice.57), channel_id=1, source_target_pairs={{0,4},{4,8},{8,12},{12,0},{1,5},{5,9},{9,13},{13,1},{2,6},{6,10},{... | collective-permute-start | bytes 49160 | tf_op jit(solution)/shard_map/ppermute | solution.py:17
  29.8 1.6 %copy-start.5 = (bf16[512,2048]{1,0:T(8,128)(2,1)S(1)}, bf16[512,2048]{1,0:T(8,128)(2,1)}, u32[]{:S(2)}) copy-start(bf16[512,2048]{1,0:T(8,128)(2,1)} %branch_hbm.1) | copy-start | bytes 6291460
  31.4 1.0 %copy-start.6 = (bf16[16,128,128]{2,1,0:T(8,128)(2,1)S(1)}, bf16[16,128,128]{2,1,0:T(8,128)(2,1)}, u32[]{:S(2)}) copy-start(bf16[16,128,128]{2,1,0:T(8,128)(2,1)} %group_hbm.1) | copy-start | bytes 1572868
  32.5 0.9 %copy-start.8 = (bf16[256,512]{1,0:T(8,128)(2,1)S(1)}, bf16[256,512]{1,0:T(8,128)(2,1)}, u32[]{:S(2)}) copy-start(bf16[256,512]{1,0:T(8,128)(2,1)} %x_hbm.1) | copy-start | bytes 786436
  33.4 0.7 copy-start.10
  36.3 11.3 %collective-permute-start.1 = (bf16[2,256,512]{2,1,0:T(8,128)(2,1)S(1)}, bf16[2,256,512]{2,1,0:T(8,128)(2,1)S(1)}, u32[]{:S(2)}, u32[]{:S(2)}) collective-permute-start(bf16[2,256,512]{2,1,0:T(8,128)(2,1)S(1)} %get-tuple-element.34), channel_id=1, source_target_pairs={{0,1},{1,0},{2,3},{3,2},{4,5},{5,4},{6,7},{7,6},{8,9},{9,8},{10,11... | collective-permute-start | bytes 1572872 | tf_op jit(solution)/shard_map/ppermute | solution.py:22
  36.4 2.0 %copy-start.3 = (bf16[1,2048,896]{2,1,0:T(8,128)(2,1)S(1)}, bf16[1,2048,896]{2,1,0:T(8,128)(2,1)}, u32[]{:S(2)}) copy-start(bf16[1,2048,896]{2,1,0:T(8,128)(2,1)} %refs_1_.1) | copy-start | bytes 11010052
  38.4 2.0 %copy-start.4 = (bf16[1,896,2048]{2,1,0:T(8,128)(2,1)S(1)}, bf16[1,896,2048]{2,1,0:T(8,128)(2,1)}, u32[]{:S(2)}) copy-start(bf16[1,896,2048]{2,1,0:T(8,128)(2,1)} %refs_2_.1) | copy-start | bytes 11010052
  41.3 2.4 %copy-start = (bf16[1,896,2048]{2,1,0:T(8,128)(2,1)}, bf16[1,896,2048]{2,1,0:T(8,128)(2,1)S(1)}, u32[]{:S(2)}) copy-start(bf16[1,896,2048]{2,1,0:T(8,128)(2,1)S(1)} %get-tuple-element.47.down_ref) | copy-start | bytes 11010052
  43.6 6.3 %copy-start.12 = (s32[128,2]{0,1:T(2,128)S(1)}, s32[128,2]{0,1:T(2,128)}, u32[]{:S(2)}) copy-start(s32[128,2]{0,1:T(2,128)} %param.17) | copy-start | bytes 3076
  43.6 7.4 %copy-start.14 = (f32[128,2]{0,1:T(2,128)S(1)}, f32[128,2]{0,1:T(2,128)}, u32[]{:S(2)}) copy-start(f32[128,2]{0,1:T(2,128)} %param.18) | copy-start | bytes 3076
  47.0 15.1 %collective-permute-start.7 = (bf16[2,384,512]{2,1,0:T(8,128)(2,1)S(1)}, bf16[2,384,512]{2,1,0:T(8,128)(2,1)S(1)}, u32[]{:S(2)}, u32[]{:S(2)}) collective-permute-start(bf16[2,384,512]{2,1,0:T(8,128)(2,1)S(1)} %get-tuple-element.49), channel_id=1, source_target_pairs={{0,1},{1,0},{2,3},{3,2},{4,5},{5,4},{6,7},{7,6},{8,9},{9,8},{10,11... | collective-permute-start | bytes 2359304 | tf_op jit(solution)/shard_map/ppermute | solution.py:22
  47.6 0.8 copy-start.13
  48.4 8.4 %collective-permute-start.2 = (bf16[256,512]{1,0:T(8,128)(2,1)S(1)}, bf16[256,512]{1,0:T(8,128)(2,1)}, u32[]{:S(2)}, u32[]{:S(2)}) collective-permute-start(bf16[256,512]{1,0:T(8,128)(2,1)S(1)} %fusion.3), channel_id=1, source_target_pairs={{0,2},{1,3},{2,0},{3,1},{4,6},{5,7},{6,4},{7,5},{8,10},{9,11},{10,... | collective-permute-start | bytes 786440 | tf_op jit(solution)/shard_map/ppermute | solution.py:17
  58.6 2.0 %copy-start.1 = (bf16[1,896,2048]{2,1,0:T(8,128)(2,1)S(1)}, bf16[1,896,2048]{2,1,0:T(8,128)(2,1)}, u32[]{:S(2)}) copy-start(bf16[1,896,2048]{2,1,0:T(8,128)(2,1)} %copy-done) | copy-start | bytes 11010052
  62.2 13.7 %collective-permute-start.13 = (bf16[96,512]{1,0:T(8,128)(2,1)S(1)}, bf16[96,512]{1,0:T(8,128)(2,1)S(1)}, u32[]{:S(2)}, u32[]{:S(2)}) collective-permute-start(bf16[96,512]{1,0:T(8,128)(2,1)S(1)} %fusion.11), channel_id=1, source_target_pairs={{0,2},{1,3},{2,0},{3,1},{4,6},{5,7},{6,4},{7,5},{8,10},{9,11},{10,... | collective-permute-start | bytes 294920 | tf_op jit(solution)/shard_map/ppermute | solution.py:17
  63.9 6.2 %collective-permute-start.8 = (bf16[96,512]{1,0:T(8,128)(2,1)S(1)}, bf16[96,512]{1,0:T(8,128)(2,1)S(1)}, u32[]{:S(2)}, u32[]{:S(2)}) collective-permute-start(bf16[96,512]{1,0:T(8,128)(2,1)S(1)} %fusion.9), channel_id=1, source_target_pairs={{0,2},{1,3},{2,0},{3,1},{4,6},{5,7},{6,4},{7,5},{8,10},{9,11},{10,... | collective-permute-start | bytes 294920 | tf_op jit(solution)/shard_map/ppermute | solution.py:17
  64.5 9.2 %collective-permute-start.10 = (bf16[192,512]{1,0:T(8,128)(2,1)S(1)}, bf16[192,512]{1,0:T(8,128)(2,1)S(1)}, u32[]{:S(2)}, u32[]{:S(2)}) collective-permute-start(bf16[192,512]{1,0:T(8,128)(2,1)S(1)} %fusion.5), channel_id=1, source_target_pairs={{0,2},{1,3},{2,0},{3,1},{4,6},{5,7},{6,4},{7,5},{8,10},{9,11},{10,... | collective-permute-start | bytes 589832 | tf_op jit(solution)/shard_map/ppermute | solution.py:17
  70.1 7.6 %collective-permute-start.9 = (bf16[96,512]{1,0:T(8,128)(2,1)S(1)}, bf16[96,512]{1,0:T(8,128)(2,1)S(1)}, u32[]{:S(2)}, u32[]{:S(2)}) collective-permute-start(bf16[96,512]{1,0:T(8,128)(2,1)S(1)} %fusion.7), channel_id=1, source_target_pairs={{0,8},{4,12},{8,0},{12,4},{1,9},{5,13},{9,1},{13,5},{2,10},{6,14},... | collective-permute-start | bytes 294920 | tf_op jit(solution)/shard_map/ppermute | solution.py:17
  73.8 5.1 %collective-permute-start.11 = (bf16[96,512]{1,0:T(8,128)(2,1)S(1)}, bf16[96,512]{1,0:T(8,128)(2,1)S(1)}, u32[]{:S(2)}, u32[]{:S(2)}) collective-permute-start(bf16[96,512]{1,0:T(8,128)(2,1)S(1)} %get-tuple-element.55), channel_id=1, source_target_pairs={{0,12},{4,0},{8,4},{12,8},{1,13},{5,1},{9,5},{13,9},{2,14},{6,2},{... | collective-permute-start | bytes 294920 | tf_op jit(solution)/shard_map/ppermute | solution.py:17
  75.9 6.4 %collective-permute-start.12 = (bf16[96,512]{1,0:T(8,128)(2,1)S(1)}, bf16[96,512]{1,0:T(8,128)(2,1)S(1)}, u32[]{:S(2)}, u32[]{:S(2)}) collective-permute-start(bf16[96,512]{1,0:T(8,128)(2,1)S(1)} %get-tuple-element.54), channel_id=1, source_target_pairs={{0,4},{4,8},{8,12},{12,0},{1,5},{5,9},{9,13},{13,1},{2,6},{6,10},{... | collective-permute-start | bytes 294920 | tf_op jit(solution)/shard_map/ppermute | solution.py:17
